TPU v7x, 32 devices: a whole 2x2x4 slice. The times are simulated.
32 devices in a mesh: fs: 8 (over z, x), tp: 4 (over y, core).
Axes of the slice: x: 2, y: 2, z: 4, core: 2. Of those that a mesh axis runs over, the one named last changes fastest.
Arguments:
- stream: bfloat16 [4096, 2048], P('fs', 'tp'), may hold values from -6 to 6
- gain_mix: float32 [2048], replicated, may hold values from 0.1 to 1.9
- pool_weight: bfloat16 [4, 512, 512], P(None, 'fs', 'tp'), may hold values from -0.25 to 0.25
- pool_gain: float32 [2048], replicated, may hold values from 0.1 to 1.9
- gain_ffn: float32 [2048], replicated, may hold values from 0.1 to 1.9
- gate_weight: bfloat16 [2048, 5632], P('fs', 'tp'), may hold values from -0.125 to 0.125
- up_weight: bfloat16 [2048, 5632], P('fs', 'tp'), may hold values from -0.125 to 0.125
- gate_taps: float32 [3, 5632], replicated, may hold values from -2.5 to 2.5
- up_taps: float32 [3, 5632], replicated, may hold values from -2.5 to 2.5
- down_weight: bfloat16 [5632, 2048], P('tp', 'fs'), may hold values from -0.078125 to 0.078125
Outputs:
- layer_out: bfloat16 [4096, 2048], P('fs', 'tp')
All inputs are finite; a program needn't handle non-finite values.
Results may differ from a plain program's by a relative error of at most 0.01.
Values may be sent and summed in bfloat16 or wider, within the bound.
A program may use at most 64 MiB of HBM per device.

v0:
```python
import jax
import jax.numpy as jnp
from jax import lax
from jax.sharding import PartitionSpec as P

LEN = 128
epsilon = 1e-06


def rms_norm(values, scales):
    return values * lax.rsqrt(jnp.mean(values * values, axis=-1, keepdims=True) + epsilon) * scales


def delayed(values, amount):
    return jnp.pad(values, ((0, 0), (amount, 0), (0, 0)))[:, : values.shape[1]]


def pool_less(values):
    channels = values.shape[2]
    group_id = jnp.arange(channels) % 4
    partials = [values]
    running = values
    for amount in (1, 2, 4, 8):
        running = running + delayed(running, amount)
        partials.append(running)
    picked = jnp.where(
        group_id == 0,
        partials[1],
        jnp.where(group_id == 1, partials[2], jnp.where(group_id == 2, partials[3], partials[4])),
    )
    extent = jnp.where(
        group_id == 0, 2.0, jnp.where(group_id == 1, 4.0, jnp.where(group_id == 2, 8.0, 16.0))
    )
    position = jnp.arange(values.shape[1]).astype(jnp.float32)[:, None] + 1.0
    divisor = jnp.minimum(position, extent[None, :])
    return picked / divisor[None] - values


def causal_taps(values, kernel):
    reach = kernel.shape[0]
    length = values.shape[1]
    padded = jnp.pad(values, ((0, 0), (reach - 1, 0), (0, 0)))
    running = padded[:, 0:length] * kernel[0]
    for shift_by in range(1, reach):
        running = running + padded[:, shift_by : shift_by + length] * kernel[shift_by]
    return running


def add_rows(left, portion):
    return jnp.dot(left, portion, preferred_element_type=jnp.float32)


def body(
    stream,
    gain_mix,
    pool_weight,
    pool_gain,
    gain_ffn,
    gate_weight,
    up_weight,
    gate_taps,
    up_taps,
    down_weight,
):
    tok_rows, own_cols = stream.shape
    seq_count = tok_rows // LEN
    gathered = lax.all_gather(stream, "tp", axis=1, tiled=True)
    channels = gathered.shape[1]
    normed = lax.optimization_barrier(
        rms_norm(gathered.astype(jnp.float32), gain_mix).astype(jnp.bfloat16)
    )
    pooled = pool_less(normed.astype(jnp.float32).reshape(seq_count, LEN, channels)).astype(
        jnp.bfloat16
    )
    pooled = pooled.reshape(tok_rows, channels // 4, 4)
    pool_part = lax.all_gather(pool_weight, "fs", axis=1, tiled=True)
    pool_full = lax.all_gather(pool_part, "tp", axis=2, tiled=True)
    mixer = (
        jnp.einsum("tcg,gce->teg", pooled, pool_full, preferred_element_type=jnp.float32).reshape(
            tok_rows, channels
        )
        * pool_gain
    )
    middle = lax.optimization_barrier((gathered.astype(jnp.float32) + mixer).astype(jnp.bfloat16))
    normed_ffn = rms_norm(middle.astype(jnp.float32), gain_ffn).astype(jnp.bfloat16)
    hidden_cols = gate_weight.shape[1]

    def add_single(portion):
        return add_rows(normed_ffn, portion)

    gate_sum = add_single(lax.all_gather(gate_weight, "fs", axis=0, tiled=True))
    value_sum = add_single(lax.all_gather(up_weight, "fs", axis=0, tiled=True))
    gate_proj = lax.optimization_barrier(gate_sum.astype(jnp.bfloat16))
    value_proj = lax.optimization_barrier(value_sum.astype(jnp.bfloat16))
    column_start = lax.axis_index("tp") * hidden_cols
    gate_kernel = lax.dynamic_slice_in_dim(gate_taps, column_start, hidden_cols, 1)
    value_kernel = lax.dynamic_slice_in_dim(up_taps, column_start, hidden_cols, 1)
    gate_conv = causal_taps(
        gate_proj.astype(jnp.float32).reshape(seq_count, LEN, hidden_cols), gate_kernel
    )
    value_conv = causal_taps(
        value_proj.astype(jnp.float32).reshape(seq_count, LEN, hidden_cols), value_kernel
    )
    hidden = (
        (jax.nn.silu(gate_conv) * value_conv).astype(jnp.bfloat16).reshape(tok_rows, hidden_cols)
    )
    partial_value = jnp.dot(
        hidden,
        lax.all_gather(down_weight, "fs", axis=1, tiled=True),
        preferred_element_type=jnp.float32,
    )
    return lax.psum_scatter(partial_value, "tp", scatter_dimension=1, tiled=True).astype(
        jnp.bfloat16
    )


def solution(mesh):
    return jax.shard_map(
        body,
        mesh=mesh,
        in_specs=(
            P("fs", "tp"),
            P(),
            P(None, "fs", "tp"),
            P(),
            P(),
            P("fs", "tp"),
            P("fs", "tp"),
            P(),
            P(),
            P("tp", "fs"),
        ),
        out_specs=P("fs", "tp"),
        check_vma=False,
    )
```

profile of v0, /device:TPU:0, one launch (start us, length us, event | category | flops | bytes accessed | tf_op | source)
XLA Modules:
  0.0 408.1 jit_solution(10271177089141165696)
XLA Ops:
  6.5 2.0 copy.16
  9.6 33.2 %all_gather.19 = bf16[4,512,128]{2,0,1:T(4,128)(2,1)S(1)} all-gather(bf16[4,64,128]{2,0,1:T(4,128)(2,1)S(1)} %copy.17), channel_id=1, replica_groups=mesh['fs'=8,'tp'=4] {'fs'}, dimensions={1}, use_global_device_ids=true | all-gather | bytes 589824 | tf_op jit(solution)/shard_map/all_gather | solution.py:76
  47.2 2.1 fusion.3
  49.4 2.2 fusion.5
  51.5 3.1 reshape.110
  54.6 5.6 %fusion.9 = f32[4,128,2048]{1,0,2:T(4,128)S(1)} fusion(f32[4,128,2048]{1,0,2:T(4,128)} %reshape.110), kind=kLoop, calls=%fused_computation.20 | loop fusion | flops 1048576 | bytes 8388608 | tf_op jit(solution)/shard_map/add | solution.py:24
  60.3 2.3 fusion.10
  62.6 2.3 fusion.11
  65.0 16.9 %fusion.12 = bf16[4,128,2048]{1,0,2:T(4,128)(2,1)} fusion(f32[4,128,2048]{1,0,2:T(4,128)S(1)} %copy-done, f32[4,128,2048]{1,0,2:T(4,128)S(1)} %fusion.9, f32[4,128,2048]{1,0,2:T(4,128)S(1)} %fusion.11, f32[128,2048]{0,1:T(8,128)S(1)} %broadcast_minimum_fusion, pred[2048]{0:T(1024)(128)(4,1)S(1)} %get-tuple-element.11, ...), kind=kLoop, calls=%fused_computation.23 | loop fusion | flops 8388608 | bytes 15734784 | tf_op jit(solution)/shard_map/convert_element_type | solution.py:72
  81.9 2.7 reshape.102
  84.7 3.0 convolution_bitcast_fusion
  87.7 4.8 %copy.20 = f32[512,512,4]{0,2,1:T(4,128)} copy(f32[512,512,4]{0,1,2:T(8,128)S(1)} %convolution_bitcast_fusion) | data formatting | bytes 8388608 | tf_op jit(solution)/shard_map/tcg,gce->teg/transpose | solution.py:79
  92.4 5.5 %reshape.103 = f32[512,2048]{0,1:T(8,128)} reshape(f32[512,512,4]{0,2,1:T(4,128)} %copy.20) | data formatting | bytes 8388608 | tf_op jit(solution)/shard_map/reshape | solution.py:79
  97.9 2.7 fusion.6
  100.7 1.3 copy-done.2
  102.5 59.6 %all-gather.10.cloned.1.call-done = bf16[2048,1408]{1,0:T(8,128)(2,1)} async-done(((bf16[256,1408]{1,0:T(8,128)(2,1)}), bf16[2048,1408]{1,0:T(8,128)(2,1)}) %all-gather.10.cloned.1.call-update) | async-done | bytes 5767184 | tf_op jit(solution)/shard_map/all_gather | solution.py:91
  162.1 6.9 %convolution_convert_fusion.1 = bf16[512,1408]{1,0:T(8,128)(2,1)S(1)} fusion(bf16[2048,1408]{1,0:T(8,128)(2,1)} %all-gather.10.cloned.1.call-done, bf16[512,2048]{0,1:T(8,128)(2,1)} %copy-done.2, f32[2048]{0:T(1024)S(1)} %copy-done.5, f32[512]{0:T(512)S(1)} %add_rsqrt_fusion), kind=kOutput, calls=%fused_computation.25 | convolution fusion | flops 2957705216 | bytes 9316352 | tf_op jit(solution)/shard_map/dot_general | solution.py:50
  169.2 85.4 %all-gather.12.cloned.1.call-done = bf16[2048,1408]{1,0:T(8,128)(2,1)} async-done(((bf16[256,1408]{1,0:T(8,128)(2,1)}), bf16[2048,1408]{1,0:T(8,128)(2,1)}) %all-gather.12.cloned.1.call-update) | async-done | bytes 5767184 | tf_op jit(solution)/shard_map/all_gather | solution.py:92
  254.6 6.9 %convolution_convert_fusion = bf16[512,1408]{1,0:T(8,128)(2,1)S(1)} fusion(bf16[2048,1408]{1,0:T(8,128)(2,1)} %all-gather.12.cloned.1.call-done, bf16[512,2048]{0,1:T(8,128)(2,1)} %copy-done.2, f32[2048]{0:T(1024)S(1)} %copy-done.5, f32[512]{0:T(512)S(1)} %add_rsqrt_fusion), kind=kOutput, calls=%fused_computation.24 | convolution fusion | flops 2957705216 | bytes 9316352 | tf_op jit(solution)/shard_map/dot_general | solution.py:50
  261.8 3.3 fusion.21
  265.1 82.8 %all-gather.14.cloned.1.call-done = bf16[1408,2048]{1,0:T(8,128)(2,1)} async-done(((bf16[1408,256]{1,0:T(8,128)(2,1)}), bf16[1408,2048]{1,0:T(8,128)(2,1)}) %all-gather.14.cloned.1.call-update) | async-done | bytes 5767184 | tf_op jit(solution)/shard_map/all_gather | solution.py:109
  347.9 8.5 %fusion.32 = f32[512,2048]{1,0:T(8,128)} fusion(bf16[512,1408]{1,0:T(8,128)(2,1)} %bitcast.18, bf16[1408,2048]{1,0:T(8,128)(2,1)} %all-gather.14.cloned.1.call-done), kind=kOutput, calls=%fused_computation.61 | convolution fusion | flops 2952790016 | bytes 11403264 | tf_op jit(solution)/shard_map/dot_general | solution.py:107
  356.4 42.7 %reduce-scatter.2.cloned.1.call-done = f32[512,512]{1,0:T(8,128)} async-done(((f32[512,2048]{1,0:T(8,128)}), f32[512,512]{1,0:T(8,128)}) %reduce-scatter.2.cloned.1.call-update) | async-done | bytes 1048592 | tf_op jit(solution)/shard_map/reduce_scatter | solution.py:112
  399.2 2.1 convert_element_type.62
  (38 shorter events, 6.4 us)
Async XLA Ops:
  6.5 40.7 %all-gather.6.cloned.1.call-start = ((), (), s32[]{:S(2)}) async-start(), calls=%async_computation.1 | async-start | bytes 2621440 | tf_op jit(solution)/shard_map/all_gather | solution.py:67
  8.6 40.8 %copy-start.3 = (f32[2048]{0:T(1024)S(1)}, f32[2048]{0:T(1024)}, u32[]{:S(2)}) copy-start(f32[2048]{0:T(1024)} %param.11) | copy-start | bytes 24580
  8.6 76.1 %all-gather.8.cloned.1.call-start = ((), (), s32[]{:S(2)}) async-start(), calls=%async_computation.2 | async-start | bytes 2621440 | tf_op jit(solution)/shard_map/all_gather | solution.py:77
  43.9 118.2 %all-gather.10.cloned.1.call-start = ((), (), s32[]{:S(2)}) async-start(), calls=%async_computation.3 | async-start | bytes 6488064 | tf_op jit(solution)/shard_map/all_gather | solution.py:91
  44.6 210.0 %all-gather.12.cloned.1.call-start = ((), (), s32[]{:S(2)}) async-start(), calls=%async_computation.4 | async-start | bytes 6488064 | tf_op jit(solution)/shard_map/all_gather | solution.py:92
  45.2 302.7 %all-gather.14.cloned.1.call-start = ((), (), s32[]{:S(2)}) async-start(), calls=%async_computation.5 | async-start | bytes 6488064 | tf_op jit(solution)/shard_map/all_gather | solution.py:109
  45.8 353.4 %reduce-scatter.2.cloned.1.call-start = ((), (), s32[]{:S(2)}) async-start(), calls=%async_computation.6 | async-start | bytes 5242880 | tf_op jit(solution)/shard_map/reduce_scatter | solution.py:112
  62.6 2.3 copy-start
  92.4 5.5 %copy-start.1 = (bf16[512,2048]{0,1:T(8,128)(2,1)S(1)}, bf16[512,2048]{0,1:T(8,128)(2,1)}, u32[]{:S(2)}) copy-start(bf16[512,2048]{0,1:T(8,128)(2,1)} %all-gather.6.cloned.1.call-done) | copy-start | bytes 6291460
  92.4 5.5 %copy-start.4 = (f32[2048]{0:T(1024)S(1)}, f32[2048]{0:T(1024)}, u32[]{:S(2)}) copy-start(f32[2048]{0:T(1024)} %param.13) | copy-start | bytes 24580
  97.9 64.2 %copy-start.5 = (f32[2048]{0:T(1024)S(1)}, f32[2048]{0:T(1024)}, u32[]{:S(2)}) copy-start(f32[2048]{0:T(1024)} %param.14) | copy-start | bytes 24580
  100.7 1.3 copy-start.2
Sparse Core Ops, SparseCore 0:
  8.9 25.2 all-gather.5
  44.0 23.5 all-gather.7
  69.7 92.2 all-gather.9
  164.1 90.4 all-gather.11
  256.5 91.2 all-gather.13
  356.5 42.5 reduce-scatter.1
where the time goes:
time: 409 us; the launch traced here: 408 us
  waiting for transfers between devices  272 us (67%)
  other arithmetic  41 us (10%)
  blocking collectives  33.2 us (8%)
  matrix products  25.3 us (6%)
  local copies, waits for them, and re-layouts  22.5 us (6%)
  between operations  13.6 us (3%)
    all_gather x1, waiting for transfers between devices, body(): value_sum = add_single(lax.all_gather(up_weight, 'fs', axis=0, tiled=True))  85.4 us
    all_gather x1, waiting for transfers between devices, body(): lax.all_gather(down_weight, 'fs', axis=1, tiled=True)  82.8 us
    all_gather x1, waiting for transfers between devices, body(): gate_sum = add_single(lax.all_gather(gate_weight, 'fs', axis=0, tiled=True))  59.6 us
    reduce_scatter x1, waiting for transfers between devices, body(): lax.psum_scatter(partial_value, 'tp', scatter_dimension=1, tiled=True)  42.7 us
    all_gather x1, blocking collectives, body(): pool_part = lax.all_gather(pool_weight, 'fs', axis=1, tiled=True)  33.2 us
    convert_element_type x1, other arithmetic, body(): pool_less(normed.astype(jnp.float32).reshape(seq_count, LEN, channels))  16.9 us
    dot_general x2, matrix products, add_rows(): return jnp.dot(left, portion, preferred_element_type=jnp.float32)  13.8 us
    add x3, other arithmetic, pool_less(): running = running + delayed(running, amount)  10.3 us
  transfers between devices with their start and end apart: 6, of which 4 were waited for; matrix products, arithmetic and copies ran while one was open for 18% of the time, Pallas kernels for 0%

commit v1 on v0

--- a/solution.py
+++ b/solution.py
@@ -5,6 +5,20 @@
 
 LEN = 128
 epsilon = 1e-06
+
+
+def on_each_block(x, axis, dim, make, out_dim):
+    ways, here, step = (lax.axis_size(axis), lax.axis_index(axis), x.shape[dim])
+    earlier, later = ([], [])
+    going_up = going_down = x
+    for far in range(ways // 2 + 1):
+        earlier.append(make(going_up, (here - far) % ways * step))
+        if 0 < far < ways - ways // 2:
+            later.append(make(going_down, (here + far) % ways * step))
+        going_up = lax.ppermute(going_up, axis, [(d, (d + 1) % ways) for d in range(ways)])
+        going_down = lax.ppermute(going_down, axis, [(d, (d - 1) % ways) for d in range(ways)])
+    line = jnp.concatenate([*earlier[::-1], *later], axis=out_dim)
+    return jnp.roll(line, (here - ways // 2) * earlier[0].shape[out_dim], axis=out_dim)
 
 
 def rms_norm(values, scales):
@@ -74,11 +88,16 @@
     )
     pooled = pooled.reshape(tok_rows, channels // 4, 4)
     pool_part = lax.all_gather(pool_weight, "fs", axis=1, tiled=True)
-    pool_full = lax.all_gather(pool_part, "tp", axis=2, tiled=True)
     mixer = (
-        jnp.einsum("tcg,gce->teg", pooled, pool_full, preferred_element_type=jnp.float32).reshape(
-            tok_rows, channels
-        )
+        on_each_block(
+            pool_part,
+            "tp",
+            2,
+            lambda part, start: jnp.einsum(
+                "tcg,gce->teg", pooled, part, preferred_element_type=jnp.float32
+            ),
+            1,
+        ).reshape(tok_rows, channels)
         * pool_gain
     )
     middle = lax.optimization_barrier((gathered.astype(jnp.float32) + mixer).astype(jnp.bfloat16))

time: 409 us -> 375 us (0.917)
  waiting for transfers between devices: 272 us -> 231 us
  matrix products: 25.3 us -> 29.7 us
    all_gather x1, waiting for transfers between devices: 59.6 us -> 8.54 us  [body(): gate_sum = add_single(lax.all_gather(gate_weight, 'fs', axis=0, tiled=True))]
    ppermute x0 -> x3, waiting for transfers between devices: none -> 9.5 us  [the longest x2 9.49 us: on_each_block(): lax.ppermute(going_up, axis, [(d, (d + 1) % ways) for d in range(ways)])]
    dynamic_slice x0 -> x2, local copies, waits for them, and re-layouts: none -> 5.16 us  [on_each_block(): jnp.roll(line, (here - ways // 2) * earlier[0].shape[out_dim], axis=out_dim)]
    transpose x1 -> x0, local copies, waits for them, and re-layouts: 4.76 us -> none  [body(): jnp.einsum('tcg,gce->teg', pooled, pool_full, preferred_element_type=jnp....]
    dot_general x1 -> x4, matrix products: 2.97 us -> 7.41 us  [body(): jnp.einsum('tcg,gce->teg', pooled, part, preferred_element_type=jnp.float32)]
  transfers between devices with their start and end apart: 6 -> 8, of which waited for: 4 -> 5; matrix products, arithmetic and copies ran while one was open for 18% -> 22% of each run, Pallas kernels for 0% -> 0%
where the time goes in v1:
time: 375 us
  waiting for transfers between devices  231 us (62%)
  other arithmetic  40.1 us (11%)
  blocking collectives  33.1 us (9%)
  matrix products  29.7 us (8%)
  local copies, waits for them, and re-layouts  25.6 us (7%)
  between operations  13.4 us (4%)
    all_gather x1, waiting for transfers between devices, body(): value_sum = add_single(lax.all_gather(up_weight, 'fs', axis=0, tiled=True))  85.6 us
    all_gather x1, waiting for transfers between devices, body(): lax.all_gather(down_weight, 'fs', axis=1, tiled=True)  82.7 us
    reduce_scatter x1, waiting for transfers between devices, body(): lax.psum_scatter(partial_value, 'tp', scatter_dimension=1, tiled=True)  42.7 us
    all_gather x1, blocking collectives, body(): pool_part = lax.all_gather(pool_weight, 'fs', axis=1, tiled=True)  33.1 us
    convert_element_type x1, other arithmetic, body(): pool_less(normed.astype(jnp.float32).reshape(seq_count, LEN, channels))  16.2 us
    dot_general x2, matrix products, add_rows(): return jnp.dot(left, portion, preferred_element_type=jnp.float32)  13.8 us
    add x3, other arithmetic, pool_less(): running = running + delayed(running, amount)  10.2 us
    ppermute x2, waiting for transfers between devices, on_each_block(): lax.ppermute(going_up, axis, [(d, (d + 1) % ways) for d in range(ways)])  9.49 us
  transfers between devices with their start and end apart: 8, of which 5 were waited for; matrix products, arithmetic and copies ran while one was open for 22% of the time, Pallas kernels for 0%

profile of v1, /device:TPU:0, one launch (start us, length us, event | category | flops | bytes accessed | tf_op | source)
XLA Modules:
  0.0 374.5 jit_solution(12065762510770101453)
XLA Ops:
  6.5 2.1 copy.21
  11.1 33.1 %all_gather.16 = bf16[4,512,128]{2,0,1:T(4,128)(2,1)S(1)} all-gather(bf16[4,64,128]{2,0,1:T(4,128)(2,1)S(1)} %copy.22), channel_id=1, replica_groups=mesh['fs'=8,'tp'=4] {'fs'}, dimensions={1}, use_global_device_ids=true | all-gather | bytes 589824 | tf_op jit(solution)/shard_map/all_gather | solution.py:90
  48.6 9.5 %collective-permute-done = bf16[4,512,128]{1,2,0:T(8,128)(2,1)} collective-permute-done((bf16[4,512,128]{1,2,0:T(8,128)(2,1)}, bf16[4,512,128]{1,2,0:T(8,128)(2,1)}, u32[]{:S(2)}, u32[]{:S(2)}) %collective-permute-start) | collective-permute-done | bytes 524320 | tf_op jit(solution)/shard_map/ppermute | solution.py:18
  58.2 2.1 fusion.3
  60.3 2.1 fusion.5
  62.5 3.0 reshape.110
  65.5 5.5 %fusion.9 = f32[4,128,2048]{1,0,2:T(4,128)S(1)} fusion(f32[4,128,2048]{1,0,2:T(4,128)} %reshape.110), kind=kLoop, calls=%fused_computation.20 | loop fusion | flops 1048576 | bytes 8388608 | tf_op jit(solution)/shard_map/add | solution.py:38
  71.0 2.3 fusion.10
  73.4 2.3 fusion.11
  75.7 16.2 %fusion.12 = bf16[4,128,2048]{1,0,2:T(4,128)(2,1)S(1)} fusion(f32[4,128,2048]{1,0,2:T(4,128)S(1)} %copy-done, f32[4,128,2048]{1,0,2:T(4,128)S(1)} %fusion.9, f32[4,128,2048]{1,0,2:T(4,128)S(1)} %fusion.11, f32[128,2048]{0,1:T(8,128)S(1)} %broadcast_minimum_fusion, pred[2048]{0:T(1024)(128)(4,1)S(1)} %get-tuple-element.19, ...), kind=kLoop, calls=%fused_computation.23 | loop fusion | flops 8388608 | bytes 15734784 | tf_op jit(solution)/shard_map/convert_element_type | solution.py:86
  91.9 2.2 reshape.102
  94.1 3.0 copy.24
  105.3 4.7 %copy.30 = f32[512,512,4]{0,2,1:T(4,128)} copy(f32[512,512,4]{0,1,2:T(8,128)S(1)} %constant_dynamic-slice_fusion) | data formatting | bytes 8388608 | tf_op jit(solution)/shard_map/jit(_roll_dynamic)/dynamic_slice | solution.py:21
  110.1 5.5 %reshape.103 = f32[512,2048]{0,1:T(8,128)} reshape(f32[512,512,4]{0,2,1:T(4,128)} %copy.30) | data formatting | bytes 8388608 | tf_op jit(solution)/shard_map/reshape | solution.py:100
  115.6 2.7 fusion.6
  120.2 8.5 %all-gather.7.cloned.1.call-done = bf16[2048,1408]{1,0:T(8,128)(2,1)} async-done(((bf16[256,1408]{1,0:T(8,128)(2,1)}), bf16[2048,1408]{1,0:T(8,128)(2,1)}) %all-gather.7.cloned.1.call-update) | async-done | bytes 5767184 | tf_op jit(solution)/shard_map/all_gather | solution.py:110
  128.7 6.9 %convolution_convert_fusion.1 = bf16[512,1408]{1,0:T(8,128)(2,1)S(1)} fusion(bf16[2048,1408]{1,0:T(8,128)(2,1)} %all-gather.7.cloned.1.call-done, bf16[512,2048]{0,1:T(8,128)(2,1)} %copy-done.2, f32[2048]{0:T(1024)S(1)} %copy-done.5, f32[512]{0:T(512)S(1)} %add_rsqrt_fusion), kind=kOutput, calls=%fused_computation.25 | convolution fusion | flops 2957705216 | bytes 9316352 | tf_op jit(solution)/shard_map/dot_general | solution.py:64
  135.9 85.6 %all-gather.9.cloned.1.call-done = bf16[2048,1408]{1,0:T(8,128)(2,1)} async-done(((bf16[256,1408]{1,0:T(8,128)(2,1)}), bf16[2048,1408]{1,0:T(8,128)(2,1)}) %all-gather.9.cloned.1.call-update) | async-done | bytes 5767184 | tf_op jit(solution)/shard_map/all_gather | solution.py:111
  221.4 6.9 %convolution_convert_fusion = bf16[512,1408]{1,0:T(8,128)(2,1)S(1)} fusion(bf16[2048,1408]{1,0:T(8,128)(2,1)} %all-gather.9.cloned.1.call-done, bf16[512,2048]{0,1:T(8,128)(2,1)} %copy-done.2, f32[2048]{0:T(1024)S(1)} %copy-done.5, f32[512]{0:T(512)S(1)} %add_rsqrt_fusion), kind=kOutput, calls=%fused_computation.24 | convolution fusion | flops 2957705216 | bytes 9316352 | tf_op jit(solution)/shard_map/dot_general | solution.py:64
  228.6 3.4 fusion.21
  232.0 82.7 %all-gather.11.cloned.1.call-done = bf16[1408,2048]{1,0:T(8,128)(2,1)} async-done(((bf16[1408,256]{1,0:T(8,128)(2,1)}), bf16[1408,2048]{1,0:T(8,128)(2,1)}) %all-gather.11.cloned.1.call-update) | async-done | bytes 5767184 | tf_op jit(solution)/shard_map/all_gather | solution.py:128
  314.7 8.4 %fusion.31 = f32[512,2048]{1,0:T(8,128)} fusion(bf16[512,1408]{1,0:T(8,128)(2,1)} %bitcast.31, bf16[1408,2048]{1,0:T(8,128)(2,1)} %all-gather.11.cloned.1.call-done), kind=kOutput, calls=%fused_computation.72 | convolution fusion | flops 2952790016 | bytes 11403264 | tf_op jit(solution)/shard_map/dot_general | solution.py:126
  323.2 42.7 %reduce-scatter.2.cloned.1.call-done = f32[512,512]{1,0:T(8,128)} async-done(((f32[512,2048]{1,0:T(8,128)}), f32[512,512]{1,0:T(8,128)}) %reduce-scatter.2.cloned.1.call-update) | async-done | bytes 1048592 | tf_op jit(solution)/shard_map/reduce_scatter | solution.py:131
  365.9 2.1 convert_element_type.62
  (50 shorter events, 17.3 us)
Async XLA Ops:
  6.5 53.8 %copy-start.3 = (f32[2048]{0:T(1024)S(1)}, f32[2048]{0:T(1024)}, u32[]{:S(2)}) copy-start(f32[2048]{0:T(1024)} %param.11) | copy-start | bytes 24580
  6.5 51.7 %all-gather.5.cloned.1.call-start = ((), (), s32[]{:S(2)}) async-start(), calls=%async_computation.1 | async-start | bytes 2621440 | tf_op jit(solution)/shard_map/all_gather | solution.py:81
  8.6 120.1 %all-gather.7.cloned.1.call-start = ((), (), s32[]{:S(2)}) async-start(), calls=%async_computation.2 | async-start | bytes 6488064 | tf_op jit(solution)/shard_map/all_gather | solution.py:110
  9.4 212.1 %all-gather.9.cloned.1.call-start = ((), (), s32[]{:S(2)}) async-start(), calls=%async_computation.3 | async-start | bytes 6488064 | tf_op jit(solution)/shard_map/all_gather | solution.py:111
  10.1 304.6 %all-gather.11.cloned.1.call-start = ((), (), s32[]{:S(2)}) async-start(), calls=%async_computation.4 | async-start | bytes 6488064 | tf_op jit(solution)/shard_map/all_gather | solution.py:128
  45.3 12.7 %collective-permute-start = (bf16[4,512,128]{1,2,0:T(8,128)(2,1)}, bf16[4,512,128]{1,2,0:T(8,128)(2,1)}, u32[]{:S(2)}, u32[]{:S(2)}) collective-permute-start(bf16[4,512,128]{1,2,0:T(8,128)(2,1)} %copy.23), channel_id=1, source_target_pairs={{0,1},{1,2},{2,3},{3,0},{4,5},{5,6},{6,7},{7,4},{8,9},{9,10},{10,1... | collective-permute-start | bytes 1572872 | tf_op jit(solution)/shard_map/ppermute | solution.py:18
  45.3 57.3 %collective-permute-start.2 = (bf16[4,512,128]{1,2,0:T(8,128)(2,1)}, bf16[4,512,128]{1,2,0:T(8,128)(2,1)}, u32[]{:S(2)}, u32[]{:S(2)}) collective-permute-start(bf16[4,512,128]{1,2,0:T(8,128)(2,1)} %copy.23), channel_id=1, source_target_pairs={{0,3},{1,0},{2,1},{3,2},{4,7},{5,4},{6,5},{7,6},{8,11},{9,8},{10,9... | collective-permute-start | bytes 1572872 | tf_op jit(solution)/shard_map/ppermute | solution.py:19
  47.1 318.8 %reduce-scatter.2.cloned.1.call-start = ((), (), s32[]{:S(2)}) async-start(), calls=%async_computation.5 | async-start | bytes 5242880 | tf_op jit(solution)/shard_map/reduce_scatter | solution.py:131
  58.1 39.0 %collective-permute-start.1 = (bf16[4,512,128]{1,2,0:T(8,128)(2,1)}, bf16[4,512,128]{1,2,0:T(8,128)(2,1)}, u32[]{:S(2)}, u32[]{:S(2)}) collective-permute-start(bf16[4,512,128]{1,2,0:T(8,128)(2,1)} %collective-permute-done), channel_id=1, source_target_pairs={{0,1},{1,2},{2,3},{3,0},{4,5},{5,6},{6,7},{7,4},{8,9},{9,10},{10,1... | collective-permute-start | bytes 1572872 | tf_op jit(solution)/shard_map/ppermute | solution.py:18
  73.3 2.3 copy-start
  110.0 5.5 %copy-start.1 = (bf16[512,2048]{0,1:T(8,128)(2,1)S(1)}, bf16[512,2048]{0,1:T(8,128)(2,1)}, u32[]{:S(2)}) copy-start(bf16[512,2048]{0,1:T(8,128)(2,1)} %all-gather.5.cloned.1.call-done) | copy-start | bytes 6291460
  110.0 5.5 %copy-start.4 = (f32[2048]{0:T(1024)S(1)}, f32[2048]{0:T(1024)}, u32[]{:S(2)}) copy-start(f32[2048]{0:T(1024)} %param.13) | copy-start | bytes 24580
  115.6 13.2 %copy-start.5 = (f32[2048]{0:T(1024)S(1)}, f32[2048]{0:T(1024)}, u32[]{:S(2)}) copy-start(f32[2048]{0:T(1024)} %param.14) | copy-start | bytes 24580
  118.3 1.3 copy-start.2
Sparse Core Ops, SparseCore 0:
  8.9 25.2 all-gather.4
  36.4 92.2 all-gather.6
  130.9 90.4 all-gather.8
  223.3 91.3 all-gather.10
  323.3 42.5 reduce-scatter.1
